TPU v7x, 512 devices: a whole 4x4x16 slice. The times are simulated.
512 devices in a mesh: sp: 64 (over z, y), dp: 8 (over x, core).
Axes of the slice: x: 4, y: 4, z: 16, core: 2. Of those that a mesh axis runs over, the one named last changes fastest.
Arguments:
- gate_input: bfloat16 [8, 12288, 4096], P('dp', 'sp'), may hold values from -6 to 6
- value_input: bfloat16 [8, 12288, 4096], P('dp', 'sp'), may hold values from -6 to 6
- norm_gain: float32 [4096], replicated, may hold values from 0.1 to 1.9
- norm_bias: float32 [4096], replicated, may hold values from -3 to 3
- mix_weight: bfloat16 [64, 1024, 1024], P('sp', 'dp'), may hold values from -0.1875 to 0.1875
- mix_bias: float32 [64, 1024], P('sp'), may hold values from 0.1 to 1.9
Outputs:
- gated: bfloat16 [8, 12288, 4096], P('dp', 'sp')
All inputs are finite; a program needn't handle non-finite values.
Results may differ from a plain program's by a relative error of at most 0.0053.
Values may be sent and summed in bfloat16 or wider, within the bound.
No kernel may reach another device: no remote copies, remote signals or barrier semaphores. Data moves between devices by JAX's collectives and lax.ppermute only.
A program may use at most 64 MiB of HBM per device.

v0:
```python
import jax
import jax.numpy as jnp
from jax import lax
from jax.experimental import pallas as pl
from jax.experimental.pallas import tpu as pltpu
from jax.sharding import Mesh
from jax.sharding import PartitionSpec as P

GROUP_DIM = 64
SPAN = 1024
TILE = 128
EPSILON = 1e-05
QUAD = ("x", "zr", "y")

VMEM = pl.BlockSpec(memory_space=pltpu.VMEM)
SMEM = pl.BlockSpec(memory_space=pltpu.SMEM)
HBM = pl.BlockSpec(memory_space=pltpu.HBM)


def lane_is_low(shape):
    return lax.broadcasted_iota(jnp.int32, shape, 1) < GROUP_DIM


def swap_halves(upper, lower):
    low = lane_is_low(upper.shape)
    first = jnp.where(low, upper, pltpu.roll(lower, GROUP_DIM, 1))
    second = jnp.where(low, pltpu.roll(upper, GROUP_DIM, 1), lower)
    return first, second


STEP = 16


def row_pieces(rows):
    half = rows // 2
    return [(side, i) for i in range(half // STEP) for side in range(2)]


def fetch(source_ref, target_ref, sems, side, i):
    place = pl.ds(side * (source_ref.shape[0] // 2) + i * STEP, STEP)
    return pltpu.make_async_copy(source_ref.at[place], target_ref.at[place], sems.at[side, i])


def norm_kernel(value_hbm, gain_ref, bias_ref, out_ref, act_ref, value_ref, sems):
    rows, channels = value_hbm.shape
    half = rows // 2
    step = STEP
    tiles = channels // TILE
    for side, i in row_pieces(rows):
        fetch(value_hbm, value_ref, sems, side, i).start()

    def chunk(i, carry):
        top = pl.ds(pl.multiple_of(i * step, step), step)
        bottom = pl.ds(pl.multiple_of(half + i * step, step), step)
        for side in range(2):
            fetch(value_hbm, value_ref, sems, side, i).wait()
        total = jnp.zeros((2 * step, TILE), jnp.float32)
        for t in range(tiles):
            lanes = pl.ds(t * TILE, TILE)
            both = jnp.concatenate([value_ref[top, lanes], value_ref[bottom, lanes]], axis=0)
            act = jax.nn.gelu(both.astype(jnp.float32))
            act_ref[:, lanes] = act
            total = total + act
        centre = jnp.sum(total, axis=1, keepdims=True) * (1.0 / channels)
        square = jnp.zeros((2 * step, TILE), jnp.float32)
        for t in range(tiles):
            shifted = act_ref[:, pl.ds(t * TILE, TILE)] - centre
            square = square + shifted * shifted
        variance = jnp.sum(square, axis=1, keepdims=True) * (1.0 / channels)
        scale = lax.rsqrt(variance + EPSILON)
        for t in range(tiles):
            lanes = pl.ds(t * TILE, TILE)
            shifted = act_ref[:, lanes] - centre
            normed = shifted * scale * gain_ref[:, lanes] + bias_ref[:, lanes]
            first, second = swap_halves(normed[:step], normed[step:])
            out_ref[2 * t, top, :] = first.astype(out_ref.dtype)
            out_ref[2 * t + 1, top, :] = second.astype(out_ref.dtype)
        return carry

    lax.fori_loop(0, half // step, chunk, 0)


def fold_kernel(place_ref, weight_ref, excess_ref, bias_ref, out_ref):
    d = place_ref[0]
    for b in range(5):
        block = weight_ref[:, b * TILE : (b + 1) * TILE]
        if b >= 2:
            e = 4 - b
            block = jnp.where(b >= d + 2, excess_ref[:, e * TILE : (e + 1) * TILE], block)
        out_ref[b * TILE : (b + 1) * TILE, :] = block
    bias = bias_ref[pl.ds(d, 1), :]
    high = bias.astype(jnp.bfloat16).astype(jnp.float32)
    low = bias - high
    row = lax.broadcasted_iota(jnp.int32, (16, TILE), 0)
    pair = jnp.where(row == 0, high, jnp.where(row == 1, low, 0.0))
    out_ref[5 * TILE :, :] = pair.astype(out_ref.dtype)


def mix_kernel(place_ref, acts_ref, own_ref, other_ref, out_ref, weight, stack):
    column_of_x, core = place_ref[0], place_ref[1]
    pieces, half, _ = acts_ref.shape[1:]

    def unpack(k, carry):
        upper = pl.ds(pl.multiple_of(k * 2 * half, 2 * half), half)
        lower = pl.ds(pl.multiple_of(k * 2 * half + half, half), half)
        for pair in range(2):
            lanes = pl.ds(pair * TILE, TILE)
            first, second = swap_halves(
                acts_ref[2 * pair, k].astype(jnp.float32), acts_ref[2 * pair + 1, k].astype(jnp.float32)
            )
            stack[upper, lanes] = first.astype(stack.dtype)
            stack[lower, lanes] = second.astype(stack.dtype)
        return carry

    lax.fori_loop(0, pieces, unpack, 0)

    below = lax.broadcasted_iota(jnp.int32, (TILE, TILE), 1) <= lax.broadcasted_iota(jnp.int32, (TILE, TILE), 0)
    row8 = lax.broadcasted_iota(jnp.int32, (8, TILE), 0)
    bias_rows = jnp.zeros((8, TILE), jnp.float32)
    zero = jnp.zeros((TILE, TILE), jnp.bfloat16)
    for d in range(8):
        slot = lax.rem(column_of_x - d // 2 + 4, 4)
        mine = core == d % 2

        def held(first, count):
            rows = pl.ds(first, count)
            return jnp.where(mine, own_ref[slot, rows, :].astype(jnp.float32), other_ref[slot, rows, :].astype(jnp.float32))

        for b in range(5):
            if b <= d:
                q, p = d, b
            elif b >= d + 2:
                q, p = 7 - d, 9 - b
            else:
                continue
            block = held(b * TILE, TILE)
            if p == q:
                block = jnp.where(below, block, 0.0)
            weight[q * TILE : (q + 1) * TILE, p * TILE : (p + 1) * TILE] = block.astype(jnp.bfloat16)
        for p in range(d + 1, d // 4 * 4 + 4):
            weight[d * TILE : (d + 1) * TILE, p * TILE : (p + 1) * TILE] = zero
        pair = held(5 * TILE, 16)
        bias = pair[0:1, :] + pair[1:2, :]
        bias_rows = jnp.where(row8 == d, bias, bias_rows)
    bias_columns = bias_rows.T

    def block_of(n, carry):
        base = n * SPAN
        for i in (1, 0):
            depth = (i + 1) * 512
            summed = jnp.dot(
                weight[i * 512 : (i + 1) * 512, :depth],
                stack[pl.ds(pl.multiple_of(base, SPAN), depth), :],
                preferred_element_type=jnp.float32,
            )
            for h in range(4):
                d = 4 * i + h
                mixed = summed[h * TILE : (h + 1) * TILE] + bias_columns[:, d : d + 1]
                stack[pl.ds(pl.multiple_of(base + d * TILE, TILE), TILE), :] = mixed.astype(stack.dtype)
        return carry

    lax.fori_loop(0, pieces * 2 * half // SPAN, block_of, 0)

    def repack(k, carry):
        upper = pl.ds(pl.multiple_of(k * 2 * half, 2 * half), half)
        lower = pl.ds(pl.multiple_of(k * 2 * half + half, half), half)
        for pair in range(2):
            lanes = pl.ds(pair * TILE, TILE)
            first, second = swap_halves(stack[upper, lanes].astype(jnp.float32), stack[lower, lanes].astype(jnp.float32))
            out_ref[2 * pair, k] = first.astype(out_ref.dtype)
            out_ref[2 * pair + 1, k] = second.astype(out_ref.dtype)
        return carry

    lax.fori_loop(0, pieces, repack, 0)


def gate_kernel(gate_ref, mixed_ref, out_hbm, out_ref, out_sems):
    rows, channels = gate_ref.shape
    half = rows // 2
    step = STEP

    def send(side, i):
        place = pl.ds(side * half + i * step, step)
        return pltpu.make_async_copy(out_ref.at[place], out_hbm.at[place], out_sems.at[side, i])

    def chunk(i, carry):
        top = pl.ds(pl.multiple_of(i * step, step), step)
        bottom = pl.ds(pl.multiple_of(half + i * step, step), step)
        for t in range(channels // TILE):
            lanes = pl.ds(t * TILE, TILE)
            upper, lower = swap_halves(
                mixed_ref[2 * t, top, :].astype(jnp.float32), mixed_ref[2 * t + 1, top, :].astype(jnp.float32)
            )
            for place, mixed in ((top, upper), (bottom, lower)):
                act = jax.nn.gelu(gate_ref[place, lanes].astype(jnp.float32))
                out_ref[place, lanes] = (act * mixed).astype(out_ref.dtype)
        for side in range(2):
            send(side, i).start()
        return carry

    lax.fori_loop(0, half // step, chunk, 0)
    for side, i in row_pieces(rows):
        send(side, i).wait()


def call(kernel, out_shape, specs, flops, moved, scratch=(), out_spec=VMEM, limit=16):
    if out_spec is VMEM:
        out = pltpu.VMEM(out_shape, jnp.bfloat16)
    else:
        out = jax.ShapeDtypeStruct(out_shape, jnp.bfloat16)
    return pl.pallas_call(
        kernel,
        out_shape=out,
        in_specs=specs,
        out_specs=out_spec,
        scratch_shapes=list(scratch),
        cost_estimate=pl.CostEstimate(flops=flops, bytes_accessed=moved, transcendentals=0),
        compiler_params=pltpu.CompilerParams(vmem_limit_bytes=limit << 20),
    )


def near(array):
    return pltpu.with_memory_space_constraint(array, pltpu.VMEM)


def copy_slots(rows):
    return pltpu.SemaphoreType.DMA((2, rows // 2 // STEP))


def local(gate_input, value_input, norm_gain, norm_bias, mix_weight, mix_bias):
    _, rows, channels = value_input.shape
    groups = channels // GROUP_DIM
    half = rows // 2
    x, core = lax.axis_index("x"), lax.axis_index("core")

    weight = mix_weight[0]
    excess = lax.ppermute(weight[:, 5 * TILE :], ("x", "core"), [(5, 2), (6, 1), (7, 0)])
    place = jnp.stack([2 * x + core]).astype(jnp.int32)
    folded = call(fold_kernel, (5 * TILE + 16, TILE), [SMEM, VMEM, VMEM, VMEM], 1000000, 600000)(
        place, weight, excess, mix_bias.reshape(SPAN // TILE, TILE)
    )
    quads = lax.all_gather(folded, "zq", axis=0)
    normed = call(
        norm_kernel,
        (groups, half, TILE),
        [HBM, VMEM, VMEM],
        40000000,
        3200000,
        [pltpu.VMEM((32, channels), jnp.float32), pltpu.VMEM((rows, channels), jnp.bfloat16), copy_slots(rows)],
        limit=60,
    )(value_input[0], norm_gain.reshape(1, channels), norm_bias.reshape(1, channels))
    normed, quads = lax.optimization_barrier((normed, quads))
    acts = lax.all_to_all(normed, QUAD, split_axis=0, concat_axis=0, tiled=True)

    received = []
    for s in range(4):
        piece = lax.dynamic_index_in_dim(quads, lax.rem(x + s, 4), 0, keepdims=False)
        received.append(lax.ppermute(piece, "x", [(i, (i + s) % 4) for i in range(4)]) if s else piece)
    own = jnp.stack(received)
    other = lax.ppermute(own, "core", [(0, 1), (1, 0)])

    mixed = call(
        mix_kernel,
        (4, groups // 4, half, TILE),
        [SMEM, VMEM, VMEM, VMEM],
        1000000000,
        6000000,
        [pltpu.VMEM((SPAN, SPAN), jnp.bfloat16), pltpu.VMEM((groups // 4 * rows, 2 * TILE), jnp.bfloat16)],
    )(jnp.stack([x, core]).astype(jnp.int32), near(acts.reshape(4, groups // 4, half, TILE)), near(own), near(other))
    returned = lax.all_to_all(mixed.reshape(groups, half, TILE), QUAD, split_axis=0, concat_axis=0, tiled=True)

    gated = call(
        gate_kernel,
        (rows, channels),
        [VMEM, VMEM],
        40000000,
        4800000,
        [pltpu.VMEM((rows, channels), jnp.bfloat16), copy_slots(rows)],
        HBM,
    )(near(gate_input[0]), near(returned))
    return gated[None]


def solution(mesh):
    devices = mesh.devices.reshape(4, 4, 4, 4, 2)
    split = Mesh(devices, ("zq", "zr", "y", "x", "core"))
    sp, dp = ("zq", "zr", "y"), ("x", "core")
    in_specs = (P(dp, sp, None), P(dp, sp, None), P(), P(), P(sp, dp, None), P(sp, None))
    return jax.shard_map(local, mesh=split, in_specs=in_specs, out_specs=P(dp, sp, None), check_vma=False)
```

profile of v0, /device:TPU:8, one launch (start us, length us, event | category | flops | bytes accessed | tf_op | source)
XLA Modules:
  0.0 149.6 jit_solution(11305919384903989991)
XLA Ops:
  0.0 0.9 slice.4
  0.9 1.3 collective-permute-start
  2.2 0.0 copy-start.1
  2.2 0.0 copy-start.2
  2.2 6.2 %shard_map.64 = bf16[64,96,128]{2,1,0:T(8,128)(2,1)} custom-call(bf16[192,4096]{1,0:T(8,128)(2,1)} %bitcast.29, f32[1,4096]{1,0:T(1,128)} %bitcast.33, f32[1,4096]{1,0:T(1,128)} %bitcast.34), custom_call_target="tpu_custom_call" | custom-call | flops 40000000 | bytes 3200000 | tf_op jit(solution)/shard_map/pallas_call | solution.py:243
  8.5 0.6 collective-permute-done.excess_ref
  9.1 0.0 copy-done.1
  9.1 0.0 copy-done.2
  9.1 38.6 %all-gather = bf16[2624,128]{1,0:T(8,128)(2,1)S(1)} all-gather(bf16[656,128]{1,0:T(8,128)(2,1)S(1)} %shard_map.65), channel_id=2, replica_groups=mesh['zq'=4,'zr'=4,'y'=4,'x'=4,'core'=2] {'zq'}, dimensions={0}, use_global_device_ids=true | all-gather | bytes 839680 | tf_op jit(solution)/shard_map/all_gather | solution.py:242
  47.7 9.3 %all-to-all-start = ((bf16[64,96,128]{2,1,0:T(8,128)(2,1)}), bf16[64,96,128]{2,1,0:T(8,128)(2,1)S(1)}, u32[]{:S(2)}, u32[]{:S(2)}) async-start(bf16[64,96,128]{2,1,0:T(8,128)(2,1)} %shard_map.64), calls=%async_computation | async-start | bytes 3145728 | tf_op jit(solution)/shard_map/all_to_all | solution.py:253
  57.1 0.1 constant_dynamic-slice_fusion
  57.2 4.8 %collective-permute-start.3 = (bf16[656,128]{1,0:T(8,128)(2,1)S(1)}, bf16[656,128]{1,0:T(8,128)(2,1)S(1)}, u32[]{:S(2)}, u32[]{:S(2)}) collective-permute-start(bf16[656,128]{1,0:T(8,128)(2,1)S(1)} %get-tuple-element.10), channel_id=1, source_target_pairs={{0,6},{2,0},{4,2},{6,4},{1,7},{3,1},{5,3},{7,5},{8,14},{10,8},{12,... | collective-permute-start | bytes 503816 | tf_op jit(solution)/shard_map/ppermute | solution.py:258
  62.0 2.6 %collective-permute-start.2 = (bf16[656,128]{1,0:T(8,128)(2,1)S(1)}, bf16[656,128]{1,0:T(8,128)(2,1)S(1)}, u32[]{:S(2)}, u32[]{:S(2)}) collective-permute-start(bf16[656,128]{1,0:T(8,128)(2,1)S(1)} %get-tuple-element.11), channel_id=1, source_target_pairs={{0,4},{2,6},{4,0},{6,2},{1,5},{3,7},{5,1},{7,3},{8,12},{10,14},{12... | collective-permute-start | bytes 503816 | tf_op jit(solution)/shard_map/ppermute | solution.py:258
  64.5 2.9 %collective-permute-start.1 = (bf16[656,128]{1,0:T(8,128)(2,1)S(1)}, bf16[656,128]{1,0:T(8,128)(2,1)S(1)}, u32[]{:S(2)}, u32[]{:S(2)}) collective-permute-start(bf16[656,128]{1,0:T(8,128)(2,1)S(1)} %get-tuple-element.12), channel_id=1, source_target_pairs={{0,2},{2,4},{4,6},{6,0},{1,3},{3,5},{5,7},{7,1},{8,10},{10,12},{12... | collective-permute-start | bytes 503816 | tf_op jit(solution)/shard_map/ppermute | solution.py:258
  67.4 8.0 %collective-permute-done.3 = bf16[656,128]{1,0:T(8,128)(2,1)S(1)} collective-permute-done((bf16[656,128]{1,0:T(8,128)(2,1)S(1)}, bf16[656,128]{1,0:T(8,128)(2,1)S(1)}, u32[]{:S(2)}, u32[]{:S(2)}) %collective-permute-start.3) | collective-permute-done | bytes 167968 | tf_op jit(solution)/shard_map/ppermute | solution.py:258
  75.4 0.4 collective-permute-done.2
  75.8 4.2 %collective-permute-done.1 = bf16[656,128]{1,0:T(8,128)(2,1)S(1)} collective-permute-done((bf16[656,128]{1,0:T(8,128)(2,1)S(1)}, bf16[656,128]{1,0:T(8,128)(2,1)S(1)}, u32[]{:S(2)}, u32[]{:S(2)}) %collective-permute-start.1) | collective-permute-done | bytes 167968 | tf_op jit(solution)/shard_map/ppermute | solution.py:258
  80.0 0.1 pad_maximum_fusion.own_ref
  80.1 2.0 %collective-permute-start.4 = (bf16[4,656,128]{2,1,0:T(8,128)(2,1)S(1)}, bf16[4,656,128]{2,1,0:T(8,128)(2,1)S(1)}, u32[]{:S(2)}, u32[]{:S(2)}) collective-permute-start(bf16[4,656,128]{2,1,0:T(8,128)(2,1)S(1)} %pad_maximum_fusion.own_ref), channel_id=1, source_target_pairs={{0,1},{1,0},{2,3},{3,2},{4,5},{5,4},{6,7},{7,6},{8,9},{9,8},{10,11... | collective-permute-start | bytes 2015240 | tf_op jit(solution)/shard_map/ppermute | solution.py:260
  82.1 0.1 pad_add_fusion.place_ref
  82.2 1.9 %collective-permute-done.4.other_ref = bf16[4,656,128]{2,1,0:T(8,128)(2,1)S(1)} collective-permute-done((bf16[4,656,128]{2,1,0:T(8,128)(2,1)S(1)}, bf16[4,656,128]{2,1,0:T(8,128)(2,1)S(1)}, u32[]{:S(2)}, u32[]{:S(2)}) %collective-permute-start.4) | collective-permute-done | bytes 671776 | tf_op jit(solution)/shard_map/ppermute | solution.py:260
  84.1 11.1 %all-to-all-done = bf16[64,96,128]{2,1,0:T(8,128)(2,1)S(1)} async-done(((bf16[64,96,128]{2,1,0:T(8,128)(2,1)}), bf16[64,96,128]{2,1,0:T(8,128)(2,1)S(1)}, u32[]{:S(2)}, u32[]{:S(2)}) %all-to-all-start) | async-done | bytes 1572896 | tf_op jit(solution)/shard_map/all_to_all | solution.py:253
  95.2 7.1 %shard_map.66 = bf16[4,16,96,128]{3,2,1,0:T(8,128)(2,1)S(1)} custom-call(s32[2]{0:T(128)S(1)} %pad_add_fusion.place_ref, bf16[4,16,96,128]{3,2,1,0:T(8,128)(2,1)S(1)} %bitcast.22, bf16[4,656,128]{2,1,0:T(8,128)(2,1)S(1)} %pad_maximum_fusion.own_ref, bf16[4,656,128]{2,1,0:T(8,128)(2,1)S(1)} %collective-permute-done.4.other_ref), custom_call_target="tpu_custom_call" | custom-call | flops 1000000000 | bytes 6000000 | tf_op jit(solution)/shard_map/pallas_call | solution.py:262
  102.3 0.0 copy-start
  102.4 44.7 %all_to_all.10.mixed_ref = bf16[64,96,128]{2,1,0:T(8,128)(2,1)S(1)} all-to-all(bf16[64,96,128]{2,1,0:T(8,128)(2,1)S(1)} %bitcast.23), channel_id=1, replica_groups=mesh['zq'=4,'zr'=4,'y'=4,'x'=4,'core'=2] {'x','zr','y'}, dimensions={0} | all-to-all | bytes 3145728 | tf_op jit(solution)/shard_map/all_to_all | solution.py:270
  147.0 0.0 copy-done
  147.0 2.6 %shard_map.67 = bf16[192,4096]{1,0:T(8,128)(2,1)} custom-call(bf16[192,4096]{1,0:T(8,128)(2,1)S(1)} %bitcast.24, bf16[64,96,128]{2,1,0:T(8,128)(2,1)S(1)} %all_to_all.10.mixed_ref), custom_call_target="tpu_custom_call" | custom-call | flops 40000000 | bytes 4800000 | tf_op jit(solution)/shard_map/pallas_call | solution.py:272
  (1 shorter events, 0.0 us)
Async XLA Ops:
  0.9 8.2 %collective-permute-start = (bf16[128,384]{1,0:T(8,128)(2,1)S(1)}, bf16[128,384]{1,0:T(8,128)(2,1)S(1)}, u32[]{:S(2)}, u32[]{:S(2)}) collective-permute-start(bf16[128,384]{1,0:T(8,128)(2,1)S(1)} %slice.4), channel_id=1, source_target_pairs={{5,2},{6,1},{7,0},{13,10},{14,9},{15,8},{21,18},{22,17},{23,16},{2... | collective-permute-start | bytes 294920 | tf_op jit(solution)/shard_map/ppermute | solution.py:237
  2.2 6.9 %copy-start.1 = (bf16[1,128,1024]{2,1,0:T(8,128)(2,1)S(1)}, bf16[1,128,1024]{2,1,0:T(8,128)(2,1)}, u32[]{:S(2)}) copy-start(bf16[1,128,1024]{2,1,0:T(8,128)(2,1)} %param.10) | copy-start | bytes 786436
  2.2 6.9 %copy-start.2 = (f32[1,1024]{1,0:T(1,128)S(1)}, f32[1,1024]{1,0:T(1,128)}, u32[]{:S(2)}) copy-start(f32[1,1024]{1,0:T(1,128)} %param.11) | copy-start | bytes 12292
  47.7 47.5 %all-to-all-start = ((bf16[64,96,128]{2,1,0:T(8,128)(2,1)}), bf16[64,96,128]{2,1,0:T(8,128)(2,1)S(1)}, u32[]{:S(2)}, u32[]{:S(2)}) async-start(bf16[64,96,128]{2,1,0:T(8,128)(2,1)} %shard_map.64), calls=%async_computation | async-start | bytes 3145728 | tf_op jit(solution)/shard_map/all_to_all | solution.py:253
  57.2 18.2 %collective-permute-start.3 = (bf16[656,128]{1,0:T(8,128)(2,1)S(1)}, bf16[656,128]{1,0:T(8,128)(2,1)S(1)}, u32[]{:S(2)}, u32[]{:S(2)}) collective-permute-start(bf16[656,128]{1,0:T(8,128)(2,1)S(1)} %get-tuple-element.10), channel_id=1, source_target_pairs={{0,6},{2,0},{4,2},{6,4},{1,7},{3,1},{5,3},{7,5},{8,14},{10,8},{12,... | collective-permute-start | bytes 503816 | tf_op jit(solution)/shard_map/ppermute | solution.py:258
  62.0 13.8 %collective-permute-start.2 = (bf16[656,128]{1,0:T(8,128)(2,1)S(1)}, bf16[656,128]{1,0:T(8,128)(2,1)S(1)}, u32[]{:S(2)}, u32[]{:S(2)}) collective-permute-start(bf16[656,128]{1,0:T(8,128)(2,1)S(1)} %get-tuple-element.11), channel_id=1, source_target_pairs={{0,4},{2,6},{4,0},{6,2},{1,5},{3,7},{5,1},{7,3},{8,12},{10,14},{12... | collective-permute-start | bytes 503816 | tf_op jit(solution)/shard_map/ppermute | solution.py:258
  64.5 15.5 %collective-permute-start.1 = (bf16[656,128]{1,0:T(8,128)(2,1)S(1)}, bf16[656,128]{1,0:T(8,128)(2,1)S(1)}, u32[]{:S(2)}, u32[]{:S(2)}) collective-permute-start(bf16[656,128]{1,0:T(8,128)(2,1)S(1)} %get-tuple-element.12), channel_id=1, source_target_pairs={{0,2},{2,4},{4,6},{6,0},{1,3},{3,5},{5,7},{7,1},{8,10},{10,12},{12... | collective-permute-start | bytes 503816 | tf_op jit(solution)/shard_map/ppermute | solution.py:258
  80.1 4.0 %collective-permute-start.4 = (bf16[4,656,128]{2,1,0:T(8,128)(2,1)S(1)}, bf16[4,656,128]{2,1,0:T(8,128)(2,1)S(1)}, u32[]{:S(2)}, u32[]{:S(2)}) collective-permute-start(bf16[4,656,128]{2,1,0:T(8,128)(2,1)S(1)} %pad_maximum_fusion.own_ref), channel_id=1, source_target_pairs={{0,1},{1,0},{2,3},{3,2},{4,5},{5,4},{6,7},{7,6},{8,9},{9,8},{10,11... | collective-permute-start | bytes 2015240 | tf_op jit(solution)/shard_map/ppermute | solution.py:260
  102.3 44.7 %copy-start = (bf16[1,192,4096]{2,1,0:T(8,128)(2,1)S(1)}, bf16[1,192,4096]{2,1,0:T(8,128)(2,1)}, u32[]{:S(2)}) copy-start(bf16[1,192,4096]{2,1,0:T(8,128)(2,1)} %param.6) | copy-start | bytes 4718596
where the time goes:
time: 150 us
  blocking collectives  83.3 us (56%)
  waiting for transfers between devices  26.2 us (17%)
  starting transfers between devices  22.9 us (15%)
  Pallas kernels  16 us (11%)
    all_to_all x1, blocking collectives, local(): lax.all_to_all(mixed.reshape(groups, half, TILE), QUAD, split_axis=0, con...  44.7 us
    all_gather x1, blocking collectives, local(): quads = lax.all_gather(folded, 'zq', axis=0)  38.6 us
    ppermute x3, waiting for transfers between devices, local(): lax.ppermute(piece, 'x', [(i, (i + s) % 4) for i in range(4)])  12.6 us
    all_to_all x1, waiting for transfers between devices, local(): acts = lax.all_to_all(normed, QUAD, split_axis=0, concat_axis=0, tiled=True)  11.1 us
    ppermute x3, starting transfers between devices, local(): lax.ppermute(piece, 'x', [(i, (i + s) % 4) for i in range(4)])  10.2 us
    all_to_all x1, starting transfers between devices, local(): acts = lax.all_to_all(normed, QUAD, split_axis=0, concat_axis=0, tiled=True)  9.33 us
    pallas_call x1, Pallas kernels, local(): call(mix_kernel, (4, groups // 4, half, TILE), [SMEM, VMEM, VMEM, VMEM],...  7.12 us
    pallas_call x1, Pallas kernels, local(): call(norm_kernel, (groups, half, TILE), [HBM, VMEM, VMEM], 40000000, 3200...  6.24 us
  transfers between devices with their start and end apart: 6, of which 6 were waited for; matrix products, arithmetic and copies ran while one was open for 0% of the time, Pallas kernels for 4%

commit v1 on v0

--- a/solution.py
+++ b/solution.py
@@ -10,6 +10,8 @@
 SPAN = 1024
 TILE = 128
 EPSILON = 1e-05
+HALF = TILE // 2
+HALVES = 9
 QUAD = ("x", "zr", "y")
 
 VMEM = pl.BlockSpec(memory_space=pltpu.VMEM)
@@ -80,25 +82,61 @@
     lax.fori_loop(0, half // step, chunk, 0)
 
 
+def half_of(ref, h):
+    return ref[h % 2 * HALF : (h % 2 + 1) * HALF, h // 2 * TILE : (h // 2 + 1) * TILE]
+
+
 def fold_kernel(place_ref, weight_ref, excess_ref, bias_ref, out_ref):
     d = place_ref[0]
-    for b in range(5):
-        block = weight_ref[:, b * TILE : (b + 1) * TILE]
-        if b >= 2:
-            e = 4 - b
-            block = jnp.where(b >= d + 2, excess_ref[:, e * TILE : (e + 1) * TILE], block)
-        out_ref[b * TILE : (b + 1) * TILE, :] = block
+    for h in range(HALVES):
+        block = half_of(weight_ref, h)
+        if h >= 2:
+            moved = half_of(excess_ref, 2 * HALVES - 1 - h - 8)
+            block = jnp.where(h >= 2 * d + 2, moved, block)
+        out_ref[h * HALF : (h + 1) * HALF, :] = block
     bias = bias_ref[pl.ds(d, 1), :]
     high = bias.astype(jnp.bfloat16).astype(jnp.float32)
     low = bias - high
     row = lax.broadcasted_iota(jnp.int32, (16, TILE), 0)
     pair = jnp.where(row == 0, high, jnp.where(row == 1, low, 0.0))
-    out_ref[5 * TILE :, :] = pair.astype(out_ref.dtype)
-
-
-def mix_kernel(place_ref, acts_ref, own_ref, other_ref, out_ref, weight, stack):
+    out_ref[HALVES * HALF :, :] = pair.astype(out_ref.dtype)
+
+
+def unfold_kernel(place_ref, own_ref, other_ref, weight, bias_ref):
     column_of_x, core = place_ref[0], place_ref[1]
+    row8 = lax.broadcasted_iota(jnp.int32, (8, TILE), 0)
+    column = lax.broadcasted_iota(jnp.int32, (HALF, TILE), 1)
+    line = lax.broadcasted_iota(jnp.int32, (HALF, TILE), 0)
+    bias_rows = jnp.zeros((8, TILE), jnp.float32)
+    zero = jnp.zeros((TILE, TILE), jnp.bfloat16)
+    for d in range(8):
+        slot = lax.rem(column_of_x - d // 2 + 4, 4)
+        mine = core == d % 2
+
+        def held(first, count):
+            rows = pl.ds(first, count)
+            return jnp.where(mine, own_ref[slot, rows, :].astype(jnp.float32), other_ref[slot, rows, :].astype(jnp.float32))
+
+        for h in range(HALVES):
+            block = held(h * HALF, HALF)
+            q, place = (d, h) if h <= 2 * d + 1 else (7 - d, 2 * HALVES - 1 - h)
+            p, side = place // 2, place % 2
+            if p == q:
+                block = jnp.where(column <= line + side * HALF, block, 0.0)
+            first = q * TILE + side * HALF
+            weight[first : first + HALF, p * TILE : (p + 1) * TILE] = block.astype(jnp.bfloat16)
+        for p in range(d + 1, d // 4 * 4 + 4):
+            weight[d * TILE : (d + 1) * TILE, p * TILE : (p + 1) * TILE] = zero
+        pair = held(HALVES * HALF, 16)
+        bias = pair[0:1, :] + pair[1:2, :]
+        bias_rows = jnp.where(row8 == d, bias, bias_rows)
+    bias_ref[...] = bias_rows
+
+
+def mix_kernel(acts_ref, weight_hbm, bias_ref, out_ref, weight, stack, sem):
     pieces, half, _ = acts_ref.shape[1:]
+    weight_copy = pltpu.make_async_copy(weight_hbm, weight, sem)
+    weight_copy.start()
 
     def unpack(k, carry):
         upper = pl.ds(pl.multiple_of(k * 2 * half, 2 * half), half)
@@ -112,54 +150,24 @@
             stack[lower, lanes] = second.astype(stack.dtype)
         return carry
 
-    lax.fori_loop(0, pieces, unpack, 0)
-
-    below = lax.broadcasted_iota(jnp.int32, (TILE, TILE), 1) <= lax.broadcasted_iota(jnp.int32, (TILE, TILE), 0)
-    row8 = lax.broadcasted_iota(jnp.int32, (8, TILE), 0)
-    bias_rows = jnp.zeros((8, TILE), jnp.float32)
-    zero = jnp.zeros((TILE, TILE), jnp.bfloat16)
-    for d in range(8):
-        slot = lax.rem(column_of_x - d // 2 + 4, 4)
-        mine = core == d % 2
-
-        def held(first, count):
-            rows = pl.ds(first, count)
-            return jnp.where(mine, own_ref[slot, rows, :].astype(jnp.float32), other_ref[slot, rows, :].astype(jnp.float32))
-
-        for b in range(5):
-            if b <= d:
-                q, p = d, b
-            elif b >= d + 2:
-                q, p = 7 - d, 9 - b
-            else:
-                continue
-            block = held(b * TILE, TILE)
-            if p == q:
-                block = jnp.where(below, block, 0.0)
-            weight[q * TILE : (q + 1) * TILE, p * TILE : (p + 1) * TILE] = block.astype(jnp.bfloat16)
-        for p in range(d + 1, d // 4 * 4 + 4):
-            weight[d * TILE : (d + 1) * TILE, p * TILE : (p + 1) * TILE] = zero
-        pair = held(5 * TILE, 16)
-        bias = pair[0:1, :] + pair[1:2, :]
-        bias_rows = jnp.where(row8 == d, bias, bias_rows)
-    bias_columns = bias_rows.T
-
-    def block_of(n, carry):
+    lax.fori_loop(0, pieces, unpack, 0, unroll=True)
+
+    bias_columns = bias_ref[...].T
+
+    weight_copy.wait()
+    for n in range(pieces * 2 * half // SPAN):
         base = n * SPAN
         for i in (1, 0):
             depth = (i + 1) * 512
             summed = jnp.dot(
                 weight[i * 512 : (i + 1) * 512, :depth],
-                stack[pl.ds(pl.multiple_of(base, SPAN), depth), :],
+                stack[base : base + depth, :],
                 preferred_element_type=jnp.float32,
             )
             for h in range(4):
                 d = 4 * i + h
                 mixed = summed[h * TILE : (h + 1) * TILE] + bias_columns[:, d : d + 1]
-                stack[pl.ds(pl.multiple_of(base + d * TILE, TILE), TILE), :] = mixed.astype(stack.dtype)
-        return carry
-
-    lax.fori_loop(0, pieces * 2 * half // SPAN, block_of, 0)
+                stack[base + d * TILE : base + (d + 1) * TILE, :] = mixed.astype(stack.dtype)
 
     def repack(k, carry):
         upper = pl.ds(pl.multiple_of(k * 2 * half, 2 * half), half)
@@ -171,7 +179,7 @@
             out_ref[2 * pair + 1, k] = second.astype(out_ref.dtype)
         return carry
 
-    lax.fori_loop(0, pieces, repack, 0)
+    lax.fori_loop(0, pieces, repack, 0, unroll=True)
 
 
 def gate_kernel(gate_ref, mixed_ref, out_hbm, out_ref, out_sems):
@@ -234,9 +242,9 @@
     x, core = lax.axis_index("x"), lax.axis_index("core")
 
     weight = mix_weight[0]
-    excess = lax.ppermute(weight[:, 5 * TILE :], ("x", "core"), [(5, 2), (6, 1), (7, 0)])
+    excess = lax.ppermute(weight[:, 4 * TILE :], ("x", "core"), [(4, 3), (5, 2), (6, 1), (7, 0)])
     place = jnp.stack([2 * x + core]).astype(jnp.int32)
-    folded = call(fold_kernel, (5 * TILE + 16, TILE), [SMEM, VMEM, VMEM, VMEM], 1000000, 600000)(
+    folded = call(fold_kernel, (HALVES * HALF + 16, TILE), [SMEM, VMEM, VMEM, VMEM], 1000000, 600000)(
         place, weight, excess, mix_bias.reshape(SPAN // TILE, TILE)
     )
     quads = lax.all_gather(folded, "zq", axis=0)
@@ -259,14 +267,27 @@
     own = jnp.stack(received)
     other = lax.ppermute(own, "core", [(0, 1), (1, 0)])
 
+    full, bias_rows = pl.pallas_call(
+        unfold_kernel,
+        name="unfold",
+        out_shape=(jax.ShapeDtypeStruct((SPAN, SPAN), jnp.bfloat16), pltpu.VMEM((8, TILE), jnp.float32)),
+        in_specs=[SMEM, VMEM, VMEM],
+        out_specs=(VMEM, VMEM),
+        cost_estimate=pl.CostEstimate(flops=5000000, bytes_accessed=4000000, transcendentals=0),
+        compiler_params=pltpu.CompilerParams(vmem_limit_bytes=16 << 20),
+    )(jnp.stack([x, core]).astype(jnp.int32), near(own), near(other))
     mixed = call(
         mix_kernel,
         (4, groups // 4, half, TILE),
-        [SMEM, VMEM, VMEM, VMEM],
+        [VMEM, HBM, VMEM],
         1000000000,
         6000000,
-        [pltpu.VMEM((SPAN, SPAN), jnp.bfloat16), pltpu.VMEM((groups // 4 * rows, 2 * TILE), jnp.bfloat16)],
-    )(jnp.stack([x, core]).astype(jnp.int32), near(acts.reshape(4, groups // 4, half, TILE)), near(own), near(other))
+        [
+            pltpu.VMEM((SPAN, SPAN), jnp.bfloat16),
+            pltpu.VMEM((groups // 4 * rows, 2 * TILE), jnp.bfloat16),
+            pltpu.SemaphoreType.DMA(()),
+        ],
+    )(near(acts.reshape(4, groups // 4, half, TILE)), pltpu.with_memory_space_constraint(full, pltpu.HBM), near(bias_rows))
     returned = lax.all_to_all(mixed.reshape(groups, half, TILE), QUAD, split_axis=0, concat_axis=0, tiled=True)
 
     gated = call(

time: 150 us -> 144 us (0.960)
  waiting for transfers between devices: 26.2 us -> 23.3 us
  Pallas kernels: 16 us -> 13.8 us
  blocking collectives: 83.3 us -> 81.6 us
    pallas_call x2 -> x3, Pallas kernels: 7.17 us -> 4.99 us  [the longest x1 3.96 us: local(): call(mix_kernel, (4, groups // 4, half, TILE), [VMEM, HBM, VMEM], 1000000...]
    all_to_all x1, waiting for transfers between devices: 11.1 us -> 9.22 us  [local(): acts = lax.all_to_all(normed, QUAD, split_axis=0, concat_axis=0, tiled=True)]
    ppermute x3, waiting for transfers between devices: 12.6 us -> 10.8 us  [local(): lax.ppermute(piece, 'x', [(i, (i + s) % 4) for i in range(4)])]
  transfers between devices with their start and end apart: 6 -> 6, of which waited for: 6 -> 6; matrix products, arithmetic and copies ran while one was open for 0% -> 0% of each run, Pallas kernels for 4% -> 5%
where the time goes in v1:
time: 144 us; the launch traced here: 143 us
  blocking collectives  81.6 us (57%)
  waiting for transfers between devices  23.3 us (16%)
  starting transfers between devices  22.2 us (15%)
  Pallas kernels  13.8 us (10%)
  local copies, waits for them, and re-layouts  2.31 us (2%)
    all_to_all x1, blocking collectives, local(): lax.all_to_all(mixed.reshape(groups, half, TILE), QUAD, split_axis=0, con...  44.5 us
    all_gather x1, blocking collectives, local(): quads = lax.all_gather(folded, 'zq', axis=0)  37.1 us
    ppermute x3, waiting for transfers between devices, local(): lax.ppermute(piece, 'x', [(i, (i + s) % 4) for i in range(4)])  10.8 us
    ppermute x3, starting transfers between devices, local(): lax.ppermute(piece, 'x', [(i, (i + s) % 4) for i in range(4)])  10.2 us
    all_to_all x1, waiting for transfers between devices, local(): acts = lax.all_to_all(normed, QUAD, split_axis=0, concat_axis=0, tiled=True)  9.22 us
    all_to_all x1, starting transfers between devices, local(): acts = lax.all_to_all(normed, QUAD, split_axis=0, concat_axis=0, tiled=True)  8.72 us
    pallas_call x1, Pallas kernels, local(): call(norm_kernel, (groups, half, TILE), [HBM, VMEM, VMEM], 40000000, 3200...  6.24 us
    pallas_call x1, Pallas kernels, local(): call(mix_kernel, (4, groups // 4, half, TILE), [VMEM, HBM, VMEM], 1000000...  3.96 us
  transfers between devices with their start and end apart: 6, of which 6 were waited for; matrix products, arithmetic and copies ran while one was open for 0% of the time, Pallas kernels for 5%

profile of v1, /device:TPU:8, one launch (start us, length us, event | category | flops | bytes accessed | tf_op | source)
XLA Modules:
  0.0 143.5 jit_solution(1149268683236123329)
XLA Ops:
  0.0 0.9 slice.4
  0.9 1.3 collective-permute-start
  2.2 0.0 copy-start.2
  2.2 0.0 copy-start.3
  2.2 6.2 %shard_map.64 = bf16[64,96,128]{2,1,0:T(8,128)(2,1)} custom-call(bf16[192,4096]{1,0:T(8,128)(2,1)} %bitcast.29, f32[1,4096]{1,0:T(1,128)} %bitcast.33, f32[1,4096]{1,0:T(1,128)} %bitcast.34), custom_call_target="tpu_custom_call" | custom-call | flops 40000000 | bytes 3200000 | tf_op jit(solution)/shard_map/pallas_call | solution.py:251
  8.5 1.3 collective-permute-done.excess_ref
  9.8 0.0 copy-done.2
  9.8 0.0 copy-done.3
  9.9 37.1 %all-gather = bf16[2368,128]{1,0:T(8,128)(2,1)S(1)} all-gather(bf16[592,128]{1,0:T(8,128)(2,1)S(1)} %shard_map.65), channel_id=2, replica_groups=mesh['zq'=4,'zr'=4,'y'=4,'x'=4,'core'=2] {'zq'}, dimensions={0}, use_global_device_ids=true | all-gather | bytes 757760 | tf_op jit(solution)/shard_map/all_gather | solution.py:250
  47.0 8.7 %all-to-all-start = ((bf16[64,96,128]{2,1,0:T(8,128)(2,1)}), bf16[64,96,128]{2,1,0:T(8,128)(2,1)S(1)}, u32[]{:S(2)}, u32[]{:S(2)}) async-start(bf16[64,96,128]{2,1,0:T(8,128)(2,1)} %shard_map.64), calls=%async_computation | async-start | bytes 3145728 | tf_op jit(solution)/shard_map/all_to_all | solution.py:261
  55.7 0.1 constant_dynamic-slice_fusion
  55.8 4.8 %collective-permute-start.3 = (bf16[592,128]{1,0:T(8,128)(2,1)S(1)}, bf16[592,128]{1,0:T(8,128)(2,1)S(1)}, u32[]{:S(2)}, u32[]{:S(2)}) collective-permute-start(bf16[592,128]{1,0:T(8,128)(2,1)S(1)} %get-tuple-element.14), channel_id=1, source_target_pairs={{0,6},{2,0},{4,2},{6,4},{1,7},{3,1},{5,3},{7,5},{8,14},{10,8},{12,... | collective-permute-start | bytes 454664 | tf_op jit(solution)/shard_map/ppermute | solution.py:266
  60.6 2.6 %collective-permute-start.2 = (bf16[592,128]{1,0:T(8,128)(2,1)S(1)}, bf16[592,128]{1,0:T(8,128)(2,1)S(1)}, u32[]{:S(2)}, u32[]{:S(2)}) collective-permute-start(bf16[592,128]{1,0:T(8,128)(2,1)S(1)} %get-tuple-element.15), channel_id=1, source_target_pairs={{0,4},{2,6},{4,0},{6,2},{1,5},{3,7},{5,1},{7,3},{8,12},{10,14},{12... | collective-permute-start | bytes 454664 | tf_op jit(solution)/shard_map/ppermute | solution.py:266
  63.2 2.9 %collective-permute-start.1 = (bf16[592,128]{1,0:T(8,128)(2,1)S(1)}, bf16[592,128]{1,0:T(8,128)(2,1)S(1)}, u32[]{:S(2)}, u32[]{:S(2)}) collective-permute-start(bf16[592,128]{1,0:T(8,128)(2,1)S(1)} %get-tuple-element.16), channel_id=1, source_target_pairs={{0,2},{2,4},{4,6},{6,0},{1,3},{3,5},{5,7},{7,1},{8,10},{10,12},{12... | collective-permute-start | bytes 454664 | tf_op jit(solution)/shard_map/ppermute | solution.py:266
  66.0 7.4 %collective-permute-done.3 = bf16[592,128]{1,0:T(8,128)(2,1)S(1)} collective-permute-done((bf16[592,128]{1,0:T(8,128)(2,1)S(1)}, bf16[592,128]{1,0:T(8,128)(2,1)S(1)}, u32[]{:S(2)}, u32[]{:S(2)}) %collective-permute-start.3) | collective-permute-done | bytes 151584 | tf_op jit(solution)/shard_map/ppermute | solution.py:266
  73.5 1.0 collective-permute-done.2
  74.5 2.4 %collective-permute-done.1 = bf16[592,128]{1,0:T(8,128)(2,1)S(1)} collective-permute-done((bf16[592,128]{1,0:T(8,128)(2,1)S(1)}, bf16[592,128]{1,0:T(8,128)(2,1)S(1)}, u32[]{:S(2)}, u32[]{:S(2)}) %collective-permute-start.1) | collective-permute-done | bytes 151584 | tf_op jit(solution)/shard_map/ppermute | solution.py:266
  76.9 0.1 pad_maximum_fusion.own_ref
  77.0 1.9 %collective-permute-start.4 = (bf16[4,592,128]{2,1,0:T(8,128)(2,1)S(1)}, bf16[4,592,128]{2,1,0:T(8,128)(2,1)S(1)}, u32[]{:S(2)}, u32[]{:S(2)}) collective-permute-start(bf16[4,592,128]{2,1,0:T(8,128)(2,1)S(1)} %pad_maximum_fusion.own_ref), channel_id=1, source_target_pairs={{0,1},{1,0},{2,3},{3,2},{4,5},{5,4},{6,7},{7,6},{8,9},{9,8},{10,11... | collective-permute-start | bytes 1818632 | tf_op jit(solution)/shard_map/ppermute | solution.py:268
  78.9 0.1 pad_add_fusion.place_ref
  79.0 1.9 %collective-permute-done.4.other_ref = bf16[4,592,128]{2,1,0:T(8,128)(2,1)S(1)} collective-permute-done((bf16[4,592,128]{2,1,0:T(8,128)(2,1)S(1)}, bf16[4,592,128]{2,1,0:T(8,128)(2,1)S(1)}, u32[]{:S(2)}, u32[]{:S(2)}) %collective-permute-start.4) | collective-permute-done | bytes 606240 | tf_op jit(solution)/shard_map/ppermute | solution.py:268
  80.9 1.0 unfold.1
  81.9 0.0 copy-start
  81.9 1.3 copy-done
  83.2 9.2 %all-to-all-done = bf16[64,96,128]{2,1,0:T(8,128)(2,1)S(1)} async-done(((bf16[64,96,128]{2,1,0:T(8,128)(2,1)}), bf16[64,96,128]{2,1,0:T(8,128)(2,1)S(1)}, u32[]{:S(2)}, u32[]{:S(2)}) %all-to-all-start) | async-done | bytes 1572896 | tf_op jit(solution)/shard_map/all_to_all | solution.py:261
  92.4 4.0 %shard_map.66 = bf16[4,16,96,128]{3,2,1,0:T(8,128)(2,1)S(1)} custom-call(bf16[4,16,96,128]{3,2,1,0:T(8,128)(2,1)S(1)} %bitcast.22, bf16[1024,1024]{1,0:T(8,128)(2,1)} %copy-done, f32[8,128]{1,0:T(8,128)S(1)} %get-tuple-element.12.bias_ref), custom_call_target="tpu_custom_call" | custom-call | flops 1000000000 | bytes 6000000 | tf_op jit(solution)/shard_map/pallas_call | solution.py:279
  96.4 0.0 copy-start.1
  96.4 44.5 %all_to_all.10.mixed_ref = bf16[64,96,128]{2,1,0:T(8,128)(2,1)S(1)} all-to-all(bf16[64,96,128]{2,1,0:T(8,128)(2,1)S(1)} %bitcast.23), channel_id=1, replica_groups=mesh['zq'=4,'zr'=4,'y'=4,'x'=4,'core'=2] {'x','zr','y'}, dimensions={0} | all-to-all | bytes 3145728 | tf_op jit(solution)/shard_map/all_to_all | solution.py:291
  140.9 0.0 copy-done.1
  140.9 2.6 %shard_map.67 = bf16[192,4096]{1,0:T(8,128)(2,1)} custom-call(bf16[192,4096]{1,0:T(8,128)(2,1)S(1)} %bitcast.24, bf16[64,96,128]{2,1,0:T(8,128)(2,1)S(1)} %all_to_all.10.mixed_ref), custom_call_target="tpu_custom_call" | custom-call | flops 40000000 | bytes 4800000 | tf_op jit(solution)/shard_map/pallas_call | solution.py:293
  (1 shorter events, 0.0 us)
Async XLA Ops:
  0.9 8.9 %collective-permute-start = (bf16[128,512]{1,0:T(8,128)(2,1)S(1)}, bf16[128,512]{1,0:T(8,128)(2,1)S(1)}, u32[]{:S(2)}, u32[]{:S(2)}) collective-permute-start(bf16[128,512]{1,0:T(8,128)(2,1)S(1)} %slice.4), channel_id=1, source_target_pairs={{4,3},{5,2},{6,1},{7,0},{12,11},{13,10},{14,9},{15,8},{20,19},{21,... | collective-permute-start | bytes 393224 | tf_op jit(solution)/shard_map/ppermute | solution.py:245
  2.2 7.6 %copy-start.2 = (bf16[1,128,1024]{2,1,0:T(8,128)(2,1)S(1)}, bf16[1,128,1024]{2,1,0:T(8,128)(2,1)}, u32[]{:S(2)}) copy-start(bf16[1,128,1024]{2,1,0:T(8,128)(2,1)} %param.10) | copy-start | bytes 786436
  2.2 7.6 %copy-start.3 = (f32[1,1024]{1,0:T(1,128)S(1)}, f32[1,1024]{1,0:T(1,128)}, u32[]{:S(2)}) copy-start(f32[1,1024]{1,0:T(1,128)} %param.11) | copy-start | bytes 12292
  47.0 45.4 %all-to-all-start = ((bf16[64,96,128]{2,1,0:T(8,128)(2,1)}), bf16[64,96,128]{2,1,0:T(8,128)(2,1)S(1)}, u32[]{:S(2)}, u32[]{:S(2)}) async-start(bf16[64,96,128]{2,1,0:T(8,128)(2,1)} %shard_map.64), calls=%async_computation | async-start | bytes 3145728 | tf_op jit(solution)/shard_map/all_to_all | solution.py:261
  55.8 17.7 %collective-permute-start.3 = (bf16[592,128]{1,0:T(8,128)(2,1)S(1)}, bf16[592,128]{1,0:T(8,128)(2,1)S(1)}, u32[]{:S(2)}, u32[]{:S(2)}) collective-permute-start(bf16[592,128]{1,0:T(8,128)(2,1)S(1)} %get-tuple-element.14), channel_id=1, source_target_pairs={{0,6},{2,0},{4,2},{6,4},{1,7},{3,1},{5,3},{7,5},{8,14},{10,8},{12,... | collective-permute-start | bytes 454664 | tf_op jit(solution)/shard_map/ppermute | solution.py:266
  60.6 13.9 %collective-permute-start.2 = (bf16[592,128]{1,0:T(8,128)(2,1)S(1)}, bf16[592,128]{1,0:T(8,128)(2,1)S(1)}, u32[]{:S(2)}, u32[]{:S(2)}) collective-permute-start(bf16[592,128]{1,0:T(8,128)(2,1)S(1)} %get-tuple-element.15), channel_id=1, source_target_pairs={{0,4},{2,6},{4,0},{6,2},{1,5},{3,7},{5,1},{7,3},{8,12},{10,14},{12... | collective-permute-start | bytes 454664 | tf_op jit(solution)/shard_map/ppermute | solution.py:266
  63.2 13.7 %collective-permute-start.1 = (bf16[592,128]{1,0:T(8,128)(2,1)S(1)}, bf16[592,128]{1,0:T(8,128)(2,1)S(1)}, u32[]{:S(2)}, u32[]{:S(2)}) collective-permute-start(bf16[592,128]{1,0:T(8,128)(2,1)S(1)} %get-tuple-element.16), channel_id=1, source_target_pairs={{0,2},{2,4},{4,6},{6,0},{1,3},{3,5},{5,7},{7,1},{8,10},{10,12},{12... | collective-permute-start | bytes 454664 | tf_op jit(solution)/shard_map/ppermute | solution.py:266
  77.0 3.9 %collective-permute-start.4 = (bf16[4,592,128]{2,1,0:T(8,128)(2,1)S(1)}, bf16[4,592,128]{2,1,0:T(8,128)(2,1)S(1)}, u32[]{:S(2)}, u32[]{:S(2)}) collective-permute-start(bf16[4,592,128]{2,1,0:T(8,128)(2,1)S(1)} %pad_maximum_fusion.own_ref), channel_id=1, source_target_pairs={{0,1},{1,0},{2,3},{3,2},{4,5},{5,4},{6,7},{7,6},{8,9},{9,8},{10,11... | collective-permute-start | bytes 1818632 | tf_op jit(solution)/shard_map/ppermute | solution.py:268
  81.9 1.3 copy-start
  96.4 44.5 %copy-start.1 = (bf16[1,192,4096]{2,1,0:T(8,128)(2,1)S(1)}, bf16[1,192,4096]{2,1,0:T(8,128)(2,1)}, u32[]{:S(2)}) copy-start(bf16[1,192,4096]{2,1,0:T(8,128)(2,1)} %param.6) | copy-start | bytes 4718596

commit v2 on v1

--- a/solution.py
+++ b/solution.py
@@ -30,7 +30,7 @@
     return first, second
 
 
-STEP = 16
+STEP = 32
 
 
 def row_pieces(rows):
@@ -38,24 +38,15 @@
     return [(side, i) for i in range(half // STEP) for side in range(2)]
 
 
-def fetch(source_ref, target_ref, sems, side, i):
-    place = pl.ds(side * (source_ref.shape[0] // 2) + i * STEP, STEP)
-    return pltpu.make_async_copy(source_ref.at[place], target_ref.at[place], sems.at[side, i])
-
-
-def norm_kernel(value_hbm, gain_ref, bias_ref, out_ref, act_ref, value_ref, sems):
-    rows, channels = value_hbm.shape
+def norm_kernel(value_ref, gain_ref, bias_ref, out_ref, act_ref):
+    rows, channels = value_ref.shape
     half = rows // 2
-    step = STEP
+    step = 32
     tiles = channels // TILE
-    for side, i in row_pieces(rows):
-        fetch(value_hbm, value_ref, sems, side, i).start()
 
     def chunk(i, carry):
         top = pl.ds(pl.multiple_of(i * step, step), step)
         bottom = pl.ds(pl.multiple_of(half + i * step, step), step)
-        for side in range(2):
-            fetch(value_hbm, value_ref, sems, side, i).wait()
         total = jnp.zeros((2 * step, TILE), jnp.float32)
         for t in range(tiles):
             lanes = pl.ds(t * TILE, TILE)
@@ -251,10 +242,10 @@
     normed = call(
         norm_kernel,
         (groups, half, TILE),
-        [HBM, VMEM, VMEM],
+        [VMEM, VMEM, VMEM],
         40000000,
         3200000,
-        [pltpu.VMEM((32, channels), jnp.float32), pltpu.VMEM((rows, channels), jnp.bfloat16), copy_slots(rows)],
+        [pltpu.VMEM((64, channels), jnp.float32)],
         limit=60,
     )(value_input[0], norm_gain.reshape(1, channels), norm_bias.reshape(1, channels))
     normed, quads = lax.optimization_barrier((normed, quads))

time: 144 us -> 143 us (level)
  transfers between devices with their start and end apart: 6 -> 6, of which waited for: 6 -> 6; matrix products, arithmetic and copies ran while one was open for 0% -> 0% of each run, Pallas kernels for 5% -> 4%
where the time goes in v2:
time: 143 us; the launch traced here: 142 us
  blocking collectives  81.6 us (57%)
  waiting for transfers between devices  24.6 us (17%)
  starting transfers between devices  20.8 us (15%)
  Pallas kernels  12.5 us (9%)
  local copies, waits for them, and re-layouts  2.31 us (2%)
    all_to_all x1, blocking collectives, local(): lax.all_to_all(mixed.reshape(groups, half, TILE), QUAD, split_axis=0, con...  44.5 us
    all_gather x1, blocking collectives, local(): quads = lax.all_gather(folded, 'zq', axis=0)  37.1 us
    ppermute x3, waiting for transfers between devices, local(): lax.ppermute(piece, 'x', [(i, (i + s) % 4) for i in range(4)])  10.8 us
    ppermute x3, starting transfers between devices, local(): lax.ppermute(piece, 'x', [(i, (i + s) % 4) for i in range(4)])  10.2 us
    all_to_all x1, waiting for transfers between devices, local(): acts = lax.all_to_all(normed, QUAD, split_axis=0, concat_axis=0, tiled=True)  9.22 us
    all_to_all x1, starting transfers between devices, local(): acts = lax.all_to_all(normed, QUAD, split_axis=0, concat_axis=0, tiled=True)  7.4 us
    pallas_call x1, Pallas kernels, local(): call(norm_kernel, (groups, half, TILE), [VMEM, VMEM, VMEM], 40000000, 320...  4.94 us
    pallas_call x1, Pallas kernels, local(): call(mix_kernel, (4, groups // 4, half, TILE), [VMEM, HBM, VMEM], 1000000...  3.95 us
  transfers between devices with their start and end apart: 6, of which 6 were waited for; matrix products, arithmetic and copies ran while one was open for 0% of the time, Pallas kernels for 4%

profile of v2, /device:TPU:8, one launch (start us, length us, event | category | flops | bytes accessed | tf_op | source)
XLA Modules:
  0.0 142.1 jit_solution(3602716118217962435)
XLA Ops:
  0.0 0.9 slice.4
  0.9 1.3 collective-permute-start
  2.2 0.0 copy-start.2
  2.2 0.0 copy-start.3
  2.2 4.9 %shard_map.64 = bf16[64,96,128]{2,1,0:T(8,128)(2,1)} custom-call(bf16[192,4096]{1,0:T(8,128)(2,1)} %bitcast.29, f32[1,4096]{1,0:T(1,128)} %bitcast.33, f32[1,4096]{1,0:T(1,128)} %bitcast.34), custom_call_target="tpu_custom_call" | custom-call | flops 40000000 | bytes 3200000 | tf_op jit(solution)/shard_map/pallas_call | solution.py:242
  7.2 2.6 %collective-permute-done.excess_ref = bf16[128,512]{1,0:T(8,128)(2,1)S(1)} collective-permute-done((bf16[128,512]{1,0:T(8,128)(2,1)S(1)}, bf16[128,512]{1,0:T(8,128)(2,1)S(1)}, u32[]{:S(2)}, u32[]{:S(2)}) %collective-permute-start) | collective-permute-done | bytes 131104 | tf_op jit(solution)/shard_map/ppermute | solution.py:236
  9.8 0.0 copy-done.2
  9.8 0.0 copy-done.3
  9.9 37.1 %all-gather = bf16[2368,128]{1,0:T(8,128)(2,1)S(1)} all-gather(bf16[592,128]{1,0:T(8,128)(2,1)S(1)} %shard_map.65), channel_id=2, replica_groups=mesh['zq'=4,'zr'=4,'y'=4,'x'=4,'core'=2] {'zq'}, dimensions={0}, use_global_device_ids=true | all-gather | bytes 757760 | tf_op jit(solution)/shard_map/all_gather | solution.py:241
  47.0 7.4 %all-to-all-start = ((bf16[64,96,128]{2,1,0:T(8,128)(2,1)}), bf16[64,96,128]{2,1,0:T(8,128)(2,1)S(1)}, u32[]{:S(2)}, u32[]{:S(2)}) async-start(bf16[64,96,128]{2,1,0:T(8,128)(2,1)} %shard_map.64), calls=%async_computation | async-start | bytes 3145728 | tf_op jit(solution)/shard_map/all_to_all | solution.py:252
  54.4 0.1 constant_dynamic-slice_fusion
  54.5 4.8 %collective-permute-start.3 = (bf16[592,128]{1,0:T(8,128)(2,1)S(1)}, bf16[592,128]{1,0:T(8,128)(2,1)S(1)}, u32[]{:S(2)}, u32[]{:S(2)}) collective-permute-start(bf16[592,128]{1,0:T(8,128)(2,1)S(1)} %get-tuple-element.14), channel_id=1, source_target_pairs={{0,6},{2,0},{4,2},{6,4},{1,7},{3,1},{5,3},{7,5},{8,14},{10,8},{12,... | collective-permute-start | bytes 454664 | tf_op jit(solution)/shard_map/ppermute | solution.py:257
  59.3 2.6 %collective-permute-start.2 = (bf16[592,128]{1,0:T(8,128)(2,1)S(1)}, bf16[592,128]{1,0:T(8,128)(2,1)S(1)}, u32[]{:S(2)}, u32[]{:S(2)}) collective-permute-start(bf16[592,128]{1,0:T(8,128)(2,1)S(1)} %get-tuple-element.15), channel_id=1, source_target_pairs={{0,4},{2,6},{4,0},{6,2},{1,5},{3,7},{5,1},{7,3},{8,12},{10,14},{12... | collective-permute-start | bytes 454664 | tf_op jit(solution)/shard_map/ppermute | solution.py:257
  61.8 2.9 %collective-permute-start.1 = (bf16[592,128]{1,0:T(8,128)(2,1)S(1)}, bf16[592,128]{1,0:T(8,128)(2,1)S(1)}, u32[]{:S(2)}, u32[]{:S(2)}) collective-permute-start(bf16[592,128]{1,0:T(8,128)(2,1)S(1)} %get-tuple-element.16), channel_id=1, source_target_pairs={{0,2},{2,4},{4,6},{6,0},{1,3},{3,5},{5,7},{7,1},{8,10},{10,12},{12... | collective-permute-start | bytes 454664 | tf_op jit(solution)/shard_map/ppermute | solution.py:257
  64.7 7.4 %collective-permute-done.3 = bf16[592,128]{1,0:T(8,128)(2,1)S(1)} collective-permute-done((bf16[592,128]{1,0:T(8,128)(2,1)S(1)}, bf16[592,128]{1,0:T(8,128)(2,1)S(1)}, u32[]{:S(2)}, u32[]{:S(2)}) %collective-permute-start.3) | collective-permute-done | bytes 151584 | tf_op jit(solution)/shard_map/ppermute | solution.py:257
  72.1 1.0 collective-permute-done.2
  73.1 2.4 %collective-permute-done.1 = bf16[592,128]{1,0:T(8,128)(2,1)S(1)} collective-permute-done((bf16[592,128]{1,0:T(8,128)(2,1)S(1)}, bf16[592,128]{1,0:T(8,128)(2,1)S(1)}, u32[]{:S(2)}, u32[]{:S(2)}) %collective-permute-start.1) | collective-permute-done | bytes 151584 | tf_op jit(solution)/shard_map/ppermute | solution.py:257
  75.5 0.1 pad_maximum_fusion.own_ref
  75.6 1.9 %collective-permute-start.4 = (bf16[4,592,128]{2,1,0:T(8,128)(2,1)S(1)}, bf16[4,592,128]{2,1,0:T(8,128)(2,1)S(1)}, u32[]{:S(2)}, u32[]{:S(2)}) collective-permute-start(bf16[4,592,128]{2,1,0:T(8,128)(2,1)S(1)} %pad_maximum_fusion.own_ref), channel_id=1, source_target_pairs={{0,1},{1,0},{2,3},{3,2},{4,5},{5,4},{6,7},{7,6},{8,9},{9,8},{10,11... | collective-permute-start | bytes 1818632 | tf_op jit(solution)/shard_map/ppermute | solution.py:259
  77.6 0.1 pad_add_fusion.place_ref
  77.6 1.9 %collective-permute-done.4.other_ref = bf16[4,592,128]{2,1,0:T(8,128)(2,1)S(1)} collective-permute-done((bf16[4,592,128]{2,1,0:T(8,128)(2,1)S(1)}, bf16[4,592,128]{2,1,0:T(8,128)(2,1)S(1)}, u32[]{:S(2)}, u32[]{:S(2)}) %collective-permute-start.4) | collective-permute-done | bytes 606240 | tf_op jit(solution)/shard_map/ppermute | solution.py:259
  79.5 1.0 unfold.1
  80.5 0.0 copy-start
  80.6 1.3 copy-done
  81.9 9.2 %all-to-all-done = bf16[64,96,128]{2,1,0:T(8,128)(2,1)S(1)} async-done(((bf16[64,96,128]{2,1,0:T(8,128)(2,1)}), bf16[64,96,128]{2,1,0:T(8,128)(2,1)S(1)}, u32[]{:S(2)}, u32[]{:S(2)}) %all-to-all-start) | async-done | bytes 1572896 | tf_op jit(solution)/shard_map/all_to_all | solution.py:252
  91.1 4.0 %shard_map.66 = bf16[4,16,96,128]{3,2,1,0:T(8,128)(2,1)S(1)} custom-call(bf16[4,16,96,128]{3,2,1,0:T(8,128)(2,1)S(1)} %bitcast.22, bf16[1024,1024]{1,0:T(8,128)(2,1)} %copy-done, f32[8,128]{1,0:T(8,128)S(1)} %get-tuple-element.12.bias_ref), custom_call_target="tpu_custom_call" | custom-call | flops 1000000000 | bytes 6000000 | tf_op jit(solution)/shard_map/pallas_call | solution.py:270
  95.1 0.0 copy-start.1
  95.1 44.5 %all_to_all.10.mixed_ref = bf16[64,96,128]{2,1,0:T(8,128)(2,1)S(1)} all-to-all(bf16[64,96,128]{2,1,0:T(8,128)(2,1)S(1)} %bitcast.23), channel_id=1, replica_groups=mesh['zq'=4,'zr'=4,'y'=4,'x'=4,'core'=2] {'x','zr','y'}, dimensions={0} | all-to-all | bytes 3145728 | tf_op jit(solution)/shard_map/all_to_all | solution.py:282
  139.6 0.0 copy-done.1
  139.6 2.6 %shard_map.67 = bf16[192,4096]{1,0:T(8,128)(2,1)} custom-call(bf16[192,4096]{1,0:T(8,128)(2,1)S(1)} %bitcast.24, bf16[64,96,128]{2,1,0:T(8,128)(2,1)S(1)} %all_to_all.10.mixed_ref), custom_call_target="tpu_custom_call" | custom-call | flops 40000000 | bytes 4800000 | tf_op jit(solution)/shard_map/pallas_call | solution.py:284
  (1 shorter events, 0.0 us)
Async XLA Ops:
  0.9 8.9 %collective-permute-start = (bf16[128,512]{1,0:T(8,128)(2,1)S(1)}, bf16[128,512]{1,0:T(8,128)(2,1)S(1)}, u32[]{:S(2)}, u32[]{:S(2)}) collective-permute-start(bf16[128,512]{1,0:T(8,128)(2,1)S(1)} %slice.4), channel_id=1, source_target_pairs={{4,3},{5,2},{6,1},{7,0},{12,11},{13,10},{14,9},{15,8},{20,19},{21,... | collective-permute-start | bytes 393224 | tf_op jit(solution)/shard_map/ppermute | solution.py:236
  2.2 7.6 %copy-start.2 = (bf16[1,128,1024]{2,1,0:T(8,128)(2,1)S(1)}, bf16[1,128,1024]{2,1,0:T(8,128)(2,1)}, u32[]{:S(2)}) copy-start(bf16[1,128,1024]{2,1,0:T(8,128)(2,1)} %param.10) | copy-start | bytes 786436
  2.2 7.6 %copy-start.3 = (f32[1,1024]{1,0:T(1,128)S(1)}, f32[1,1024]{1,0:T(1,128)}, u32[]{:S(2)}) copy-start(f32[1,1024]{1,0:T(1,128)} %param.11) | copy-start | bytes 12292
  47.0 44.1 %all-to-all-start = ((bf16[64,96,128]{2,1,0:T(8,128)(2,1)}), bf16[64,96,128]{2,1,0:T(8,128)(2,1)S(1)}, u32[]{:S(2)}, u32[]{:S(2)}) async-start(bf16[64,96,128]{2,1,0:T(8,128)(2,1)} %shard_map.64), calls=%async_computation | async-start | bytes 3145728 | tf_op jit(solution)/shard_map/all_to_all | solution.py:252
  54.5 17.7 %collective-permute-start.3 = (bf16[592,128]{1,0:T(8,128)(2,1)S(1)}, bf16[592,128]{1,0:T(8,128)(2,1)S(1)}, u32[]{:S(2)}, u32[]{:S(2)}) collective-permute-start(bf16[592,128]{1,0:T(8,128)(2,1)S(1)} %get-tuple-element.14), channel_id=1, source_target_pairs={{0,6},{2,0},{4,2},{6,4},{1,7},{3,1},{5,3},{7,5},{8,14},{10,8},{12,... | collective-permute-start | bytes 454664 | tf_op jit(solution)/shard_map/ppermute | solution.py:257
  59.3 13.9 %collective-permute-start.2 = (bf16[592,128]{1,0:T(8,128)(2,1)S(1)}, bf16[592,128]{1,0:T(8,128)(2,1)S(1)}, u32[]{:S(2)}, u32[]{:S(2)}) collective-permute-start(bf16[592,128]{1,0:T(8,128)(2,1)S(1)} %get-tuple-element.15), channel_id=1, source_target_pairs={{0,4},{2,6},{4,0},{6,2},{1,5},{3,7},{5,1},{7,3},{8,12},{10,14},{12... | collective-permute-start | bytes 454664 | tf_op jit(solution)/shard_map/ppermute | solution.py:257
  61.8 13.7 %collective-permute-start.1 = (bf16[592,128]{1,0:T(8,128)(2,1)S(1)}, bf16[592,128]{1,0:T(8,128)(2,1)S(1)}, u32[]{:S(2)}, u32[]{:S(2)}) collective-permute-start(bf16[592,128]{1,0:T(8,128)(2,1)S(1)} %get-tuple-element.16), channel_id=1, source_target_pairs={{0,2},{2,4},{4,6},{6,0},{1,3},{3,5},{5,7},{7,1},{8,10},{10,12},{12... | collective-permute-start | bytes 454664 | tf_op jit(solution)/shard_map/ppermute | solution.py:257
  75.6 3.9 %collective-permute-start.4 = (bf16[4,592,128]{2,1,0:T(8,128)(2,1)S(1)}, bf16[4,592,128]{2,1,0:T(8,128)(2,1)S(1)}, u32[]{:S(2)}, u32[]{:S(2)}) collective-permute-start(bf16[4,592,128]{2,1,0:T(8,128)(2,1)S(1)} %pad_maximum_fusion.own_ref), channel_id=1, source_target_pairs={{0,1},{1,0},{2,3},{3,2},{4,5},{5,4},{6,7},{7,6},{8,9},{9,8},{10,11... | collective-permute-start | bytes 1818632 | tf_op jit(solution)/shard_map/ppermute | solution.py:259
  80.5 1.3 copy-start
  95.1 44.5 %copy-start.1 = (bf16[1,192,4096]{2,1,0:T(8,128)(2,1)S(1)}, bf16[1,192,4096]{2,1,0:T(8,128)(2,1)}, u32[]{:S(2)}) copy-start(bf16[1,192,4096]{2,1,0:T(8,128)(2,1)} %param.6) | copy-start | bytes 4718596
